TPU v7x, 32 devices: a whole 2x2x4 slice. The times are simulated.
32 devices in a mesh: fs: 4 (over z), rep: 4 (over y, x), tp: 2 (over core).
Axes of the slice: x: 2, y: 2, z: 4, core: 2. Of those that a mesh axis runs over, the one named last changes fastest.
Arguments:
- query_input: bfloat16 [16384, 4096], P(('fs', 'rep')), may hold values from -6 to 6
- query_cotangent: bfloat16 [16384, 1024], P(('fs', 'rep'), 'tp'), may hold values from -0.046875 to 0.046875
- branch_output: bfloat16 [16384, 2048], P(('fs', 'rep')), may hold values from -6 to 6
- layer_cotangent: bfloat16 [16384, 4096], P(('fs', 'rep'), 'tp'), may hold values from -0.046875 to 0.046875
- query_weight: float32 [4096, 1024], P(('rep', 'fs'), 'tp'), may hold values from -0.09375 to 0.09375
- output_weight: float32 [2048, 4096], P(('rep', 'fs'), 'tp'), may hold values from -0.125 to 0.125
- query_basis: bfloat16 [4096, 512], P(('rep', 'fs')), may hold values from -0.09375 to 0.09375
- output_basis: bfloat16 [2048, 512], P(('rep', 'fs')), may hold values from -0.125 to 0.125
- query_first: float32 [512, 1024], P(('rep', 'fs'), 'tp'), may hold values from -20 to 20
- query_second: float32 [512, 1024], P(('rep', 'fs'), 'tp'), may hold values from 0.25 to 2
- output_first: float32 [512, 4096], P(('rep', 'fs'), 'tp'), may hold values from -20 to 20
- output_second: float32 [512, 4096], P(('rep', 'fs'), 'tp'), may hold values from 0.25 to 2
Outputs:
- query_update: float32 [4096, 1024], P(('rep', 'fs'), 'tp')
- output_update: float32 [2048, 4096], P(('rep', 'fs'), 'tp')
- query_first_next: float32 [512, 1024], P(('rep', 'fs'), 'tp')
- query_second_next: float32 [512, 1024], P(('rep', 'fs'), 'tp')
- output_first_next: float32 [512, 4096], P(('rep', 'fs'), 'tp')
- output_second_next: float32 [512, 4096], P(('rep', 'fs'), 'tp')
- query_copy: bfloat16 [4096, 1024], P('rep', 'tp')
- output_copy: bfloat16 [2048, 4096], P('rep', 'tp')
All inputs are finite; a program needn't handle non-finite values.
Results may differ from a plain program's by a relative error of at most 0.0055.
Values may be sent and summed in bfloat16 or wider, within the bound.
A program may use at most 128 MiB of HBM per device.

v0:
```python
import jax
import jax.numpy as jnp
from jax import lax
from jax.sharding import PartitionSpec as P

D = 4096
QKW = 1024
R = 512


beta_first = 0.6
beta_second = 0.8
step_rate = 0.01
small_eps = 1e-06


def split_parts(values):
    upper = values.astype(jnp.bfloat16)
    lower = (values - upper.astype(jnp.float32)).astype(jnp.bfloat16)
    return (upper, lower)


def split_rows(inner, cotangent):
    upper, lower = split_parts(inner)
    dims = (((0,), (0,)), ((), ()))
    return lax.dot_general(
        upper, cotangent, dims, preferred_element_type=jnp.float32
    ) + lax.dot_general(lower, cotangent, dims, preferred_element_type=jnp.float32)


def moments(first, second, projected):
    first_next = beta_first * first + (1.0 - beta_first) * projected
    second_next = beta_second * second + (1.0 - beta_second) * projected * projected
    return (first_next, second_next, first_next / jnp.sqrt(second_next))


def body(
    query_input,
    query_cotangent,
    branch_output,
    layer_cotangent,
    query_weight,
    output_weight,
    query_basis,
    output_basis,
    query_first,
    query_second,
    output_first,
    output_second,
):
    query_whole, output_whole = (
        lax.all_gather(query_basis, ("rep", "fs"), axis=0, tiled=True),
        lax.all_gather(output_basis, ("rep", "fs"), axis=0, tiled=True),
    )
    query_inner = jnp.dot(query_input, query_whole, preferred_element_type=jnp.float32)
    output_inner = jnp.dot(branch_output, output_whole, preferred_element_type=jnp.float32)
    projected_q = lax.psum_scatter(
        split_rows(query_inner, query_cotangent), ("rep", "fs"), scatter_dimension=0, tiled=True
    )
    projected_o = lax.psum_scatter(
        split_rows(output_inner, layer_cotangent), ("rep", "fs"), scatter_dimension=0, tiled=True
    )
    first_q, second_q, normed_q = moments(query_first, query_second, projected_q)
    first_o, second_o, normed_o = moments(output_first, output_second, projected_o)
    totals = lax.psum(
        (jnp.sum(normed_q * normed_q), jnp.sum(normed_o * normed_o)), ("fs", "rep", "tp")
    )
    scale_q = lax.rsqrt(totals[0] / (R * QKW) + small_eps)
    scale_o = lax.rsqrt(totals[1] / (R * D) + small_eps)
    summed_q = jnp.dot(
        query_basis,
        lax.all_gather(normed_q.astype(jnp.bfloat16), ("rep", "fs"), axis=0, tiled=True),
        preferred_element_type=jnp.float32,
    )
    summed_o = jnp.dot(
        output_basis,
        lax.all_gather(normed_o.astype(jnp.bfloat16), ("rep", "fs"), axis=0, tiled=True),
        preferred_element_type=jnp.float32,
    )
    update_q = scale_q * summed_q
    update_o = scale_o * summed_o
    query_copy, output_copy = (
        lax.all_gather(
            (query_weight - step_rate * update_q).astype(jnp.bfloat16), "fs", axis=0, tiled=True
        ),
        lax.all_gather(
            (output_weight - step_rate * update_o).astype(jnp.bfloat16), "fs", axis=0, tiled=True
        ),
    )
    return (update_q, update_o, first_q, second_q, first_o, second_o, query_copy, output_copy)


def solution(mesh):
    in_specs = (
        P(("fs", "rep"), None),
        P(("fs", "rep"), "tp"),
        P(("fs", "rep"), None),
        P(("fs", "rep"), "tp"),
        P(("rep", "fs"), "tp"),
        P(("rep", "fs"), "tp"),
        P(("rep", "fs"), None),
        P(("rep", "fs"), None),
        P(("rep", "fs"), "tp"),
        P(("rep", "fs"), "tp"),
        P(("rep", "fs"), "tp"),
        P(("rep", "fs"), "tp"),
    )
    out_specs = (
        P(("rep", "fs"), "tp"),
        P(("rep", "fs"), "tp"),
        P(("rep", "fs"), "tp"),
        P(("rep", "fs"), "tp"),
        P(("rep", "fs"), "tp"),
        P(("rep", "fs"), "tp"),
        P("rep", "tp"),
        P("rep", "tp"),
    )
    return jax.shard_map(body, mesh=mesh, in_specs=in_specs, out_specs=out_specs, check_vma=False)
```

profile of v0, /device:TPU:0, one launch (start us, length us, event | category | flops | bytes accessed | tf_op | source)
XLA Modules:
  0.0 505.3 jit_solution(10517695907345015072)
XLA Ops:
  7.2 0.0 copy-start
  7.2 0.0 all-gather.8.cloned.1.call-start
  7.2 0.7 all-gather.8.cloned.1.call-update
  7.9 0.0 all-gather.6.cloned.1.call-start
  8.0 0.7 all-gather.6.cloned.1.call-update
  8.7 0.0 reduce-scatter.5.cloned.1.call-start
  8.7 65.3 %all-gather.8.cloned.1.call-done = bf16[2048,512]{1,0:T(8,128)(2,1)} async-done(((bf16[128,512]{1,0:T(8,128)(2,1)}), bf16[2048,512]{1,0:T(8,128)(2,1)}) %all-gather.8.cloned.1.call-update) | async-done | bytes 2097168 | tf_op jit(solution)/shard_map/all_gather | solution.py:53
  74.0 0.0 copy-start.1
  74.0 5.3 %fusion.15 = f32[1024,512]{1,0:T(8,128)S(1)} fusion(bf16[1024,2048]{1,0:T(8,128)(2,1)} %param.14, bf16[2048,512]{1,0:T(8,128)(2,1)} %all-gather.8.cloned.1.call-done), kind=kOutput, calls=%fused_computation.29 | convolution fusion | flops 2147483648 | bytes 8388608 | tf_op jit(solution)/shard_map/dot_general | solution.py:56
  79.3 0.0 copy-done.1
  79.4 2.4 fusion.3
  81.7 4.4 convolution_add_fusion
  86.1 0.0 reduce-scatter.5.cloned.1.call-update
  86.2 0.0 reduce-scatter.3.cloned.1.call-start
  86.2 65.0 %all-gather.6.cloned.1.call-done = bf16[4096,512]{1,0:T(8,128)(2,1)} async-done(((bf16[256,512]{1,0:T(8,128)(2,1)}), bf16[4096,512]{1,0:T(8,128)(2,1)}) %all-gather.6.cloned.1.call-update) | async-done | bytes 4194320 | tf_op jit(solution)/shard_map/all_gather | solution.py:52
  151.2 8.1 %fusion.14 = f32[1024,512]{1,0:T(8,128)S(1)} fusion(bf16[1024,4096]{1,0:T(8,128)(2,1)} %param.12, bf16[4096,512]{1,0:T(8,128)(2,1)} %all-gather.6.cloned.1.call-done), kind=kOutput, calls=%fused_computation.28 | convolution fusion | flops 4294967296 | bytes 14680064 | tf_op jit(solution)/shard_map/dot_general | solution.py:55
  159.3 0.0 copy-done
  159.3 0.7 fusion.6
  160.1 0.0 copy-start.9
  160.1 0.0 copy-start.10
  160.1 1.7 convolution_add_fusion.1
  161.8 0.0 copy-start.6
  161.8 0.0 copy-start.11
  161.8 0.0 copy-start.12
  161.8 0.0 reduce-scatter.3.cloned.1.call-update
  161.8 0.0 copy-start.2
  161.9 0.0 all-gather.10.cloned.1.call-start
  161.9 87.6 %reduce-scatter.5.cloned.1.call-done = f32[32,2048]{1,0:T(8,128)} async-done(((f32[512,2048]{1,0:T(8,128)}), f32[32,2048]{1,0:T(8,128)}) %reduce-scatter.5.cloned.1.call-update) | async-done | bytes 262160 | tf_op jit(solution)/shard_map/reduce_scatter | solution.py:60
  249.5 0.0 copy-done.9
  249.5 0.0 copy-done.10
  249.6 1.7 fusion.9
  251.3 0.0 copy-start.3
  251.3 0.0 copy-start.4
  251.3 0.0 all-gather.10.cloned.1.call-update
  251.3 0.0 all-gather.12.cloned.1.call-start
  251.3 0.0 copy-done.6
  251.3 0.2 copy.20
  251.5 79.1 %reduce-scatter.3.cloned.1.call-done = f32[32,512]{1,0:T(8,128)} async-done(((f32[512,512]{1,0:T(8,128)}), f32[32,512]{1,0:T(8,128)}) %reduce-scatter.3.cloned.1.call-update) | async-done | bytes 65552 | tf_op jit(solution)/shard_map/reduce_scatter | solution.py:57
  330.6 0.0 copy-done.11
  330.6 0.0 copy-done.12
  330.6 1.5 multiply_reduce_fusion.1
  332.1 0.6 copy-done.7
  332.8 0.0 copy-done.8
  332.8 43.2 %all_gather.19 = bf16[512,512]{1,0:T(8,128)(2,1)S(1)} all-gather(bf16[32,512]{1,0:T(8,128)(2,1)S(1)} %fusion.11), channel_id=1, replica_groups=mesh['fs'=4,'rep'=4,'tp'=2] {'rep','fs'}, dimensions={0}, use_global_device_ids=true | all-gather | bytes 557056 | tf_op jit(solution)/shard_map/all_gather | solution.py:72
  376.0 0.7 multiply_reduce_fusion
  376.7 37.8 %all-reduce = (f32[]{:T(128)}, f32[]{:T(128)}) all-reduce(f32[]{:T(128)} %get-tuple-element.21, f32[]{:T(128)} %multiply_reduce_fusion), channel_id=1, replica_groups=mesh['fs'=4,'rep'=4,'tp'=2] {'fs','rep','tp'}, use_global_device_ids=true, to_apply=%region_2.0 | all-reduce | flops 2 | bytes 16 | tf_op jit(solution)/shard_map/psum | solution.py:65
  415.2 0.0 copy-done.2
  415.2 0.0 copy-start.5
  415.2 1.2 subtract_convert_fusion.5
  416.4 0.0 copy-done.3
  416.4 0.0 copy-done.4
  416.4 0.0 all-gather.12.cloned.1.call-update
  416.4 0.0 all-gather.14.cloned.1.call-start
  416.5 1.6 copy.21
  418.8 0.0 all-gather.10.cloned.1.call-done
  418.8 0.0 copy-done.5
  418.8 3.1 subtract_convert_fusion.4
  421.9 0.0 all-gather.14.cloned.1.call-update
  421.9 2.0 copy.22
  424.0 23.8 %all-gather.12.cloned.1.call-done = bf16[1024,512]{0,1:T(8,128)(2,1)} async-done(((bf16[256,512]{0,1:T(8,128)(2,1)}), bf16[1024,512]{0,1:T(8,128)(2,1)}) %all-gather.12.cloned.1.call-update) | async-done | bytes 1048592 | tf_op jit(solution)/shard_map/all_gather | solution.py:83
  447.8 2.3 copy.24
  450.1 1.3 copy.23
  451.4 43.1 %all-gather.14.cloned.1.call-done = bf16[512,2048]{0,1:T(8,128)(2,1)} async-done(((bf16[128,2048]{0,1:T(8,128)(2,1)}), bf16[512,2048]{0,1:T(8,128)(2,1)}) %all-gather.14.cloned.1.call-update) | async-done | bytes 2097168 | tf_op jit(solution)/shard_map/all_gather | solution.py:86
  494.5 3.9 copy.25
  (3 shorter events, 0.0 us)
Async XLA Ops:
  7.2 152.2 %copy-start = (bf16[1024,512]{1,0:T(8,128)(2,1)S(1)}, bf16[1024,512]{1,0:T(8,128)(2,1)}, u32[]{:S(2)}) copy-start(bf16[1024,512]{1,0:T(8,128)(2,1)} %param.13) | copy-start | bytes 3145732
  7.2 66.8 %all-gather.8.cloned.1.call-start = ((), (), s32[]{:S(2)}) async-start(), calls=%async_computation.4 | async-start | bytes 2228224 | tf_op jit(solution)/shard_map/all_gather | solution.py:53
  7.9 143.3 %all-gather.6.cloned.1.call-start = ((), (), s32[]{:S(2)}) async-start(), calls=%async_computation.2 | async-start | bytes 4456448 | tf_op jit(solution)/shard_map/all_gather | solution.py:52
  8.7 240.9 %reduce-scatter.5.cloned.1.call-start = ((), (), s32[]{:S(2)}) async-start(), calls=%async_computation.5 | async-start | bytes 4456448 | tf_op jit(solution)/shard_map/reduce_scatter | solution.py:60
  74.0 5.3 %copy-start.1 = (bf16[1024,2048]{1,0:T(8,128)(2,1)S(1)}, bf16[1024,2048]{1,0:T(8,128)(2,1)}, u32[]{:S(2)}) copy-start(bf16[1024,2048]{1,0:T(8,128)(2,1)} %param.15) | copy-start | bytes 12582916
  86.2 244.5 %reduce-scatter.3.cloned.1.call-start = ((), (), s32[]{:S(2)}) async-start(), calls=%async_computation.3 | async-start | bytes 1114112 | tf_op jit(solution)/shard_map/reduce_scatter | solution.py:57
  160.1 89.5 %copy-start.9 = (f32[32,2048]{1,0:T(8,128)S(1)}, f32[32,2048]{1,0:T(8,128)}, u32[]{:S(2)}) copy-start(f32[32,2048]{1,0:T(8,128)} %param.23) | copy-start | bytes 786436
  160.1 89.5 %copy-start.10 = (f32[32,2048]{1,0:T(8,128)S(1)}, f32[32,2048]{1,0:T(8,128)}, u32[]{:S(2)}) copy-start(f32[32,2048]{1,0:T(8,128)} %param.22) | copy-start | bytes 786436
  161.8 89.5 %copy-start.6 = (f32[256,512]{1,0:T(8,128)S(1)}, f32[256,512]{1,0:T(8,128)}, u32[]{:S(2)}) copy-start(f32[256,512]{1,0:T(8,128)} %param.16) | copy-start | bytes 1572868
  161.8 168.8 %copy-start.11 = (f32[32,512]{1,0:T(8,128)S(1)}, f32[32,512]{1,0:T(8,128)}, u32[]{:S(2)}) copy-start(f32[32,512]{1,0:T(8,128)} %param.21) | copy-start | bytes 196612
  161.8 168.8 %copy-start.12 = (f32[32,512]{1,0:T(8,128)S(1)}, f32[32,512]{1,0:T(8,128)}, u32[]{:S(2)}) copy-start(f32[32,512]{1,0:T(8,128)} %param.20) | copy-start | bytes 196612
  161.8 253.3 %copy-start.2 = (bf16[256,512]{1,0:T(8,128)(2,1)S(1)}, bf16[256,512]{1,0:T(8,128)(2,1)}, u32[]{:S(2)}) copy-start(bf16[256,512]{1,0:T(8,128)(2,1)} %param.18) | copy-start | bytes 786436
  161.9 256.9 %all-gather.10.cloned.1.call-start = ((), (), s32[]{:S(2)}) async-start(), calls=%async_computation.6 | async-start | bytes 2228224 | tf_op jit(solution)/shard_map/all_gather | solution.py:77
  251.3 165.2 %copy-start.3 = (f32[32,2048]{1,0:T(8,128)}, f32[32,2048]{1,0:T(8,128)S(1)}, u32[]{:S(2)}) copy-start(f32[32,2048]{1,0:T(8,128)S(1)} %get-tuple-element.19) | copy-start | bytes 786436
  251.3 165.2 %copy-start.4 = (f32[32,2048]{1,0:T(8,128)}, f32[32,2048]{1,0:T(8,128)S(1)}, u32[]{:S(2)}) copy-start(f32[32,2048]{1,0:T(8,128)S(1)} %get-tuple-element.20) | copy-start | bytes 786436
  251.3 196.5 %all-gather.12.cloned.1.call-start = ((), (), s32[]{:S(2)}) async-start(), calls=%async_computation.7 | async-start | bytes 1310720 | tf_op jit(solution)/shard_map/all_gather | solution.py:83
  332.1 0.6 copy-start.7
  332.1 0.6 copy-start.8
  415.2 3.6 copy-start.5
  416.4 78.1 %all-gather.14.cloned.1.call-start = ((), (), s32[]{:S(2)}) async-start(), calls=%async_computation.8 | async-start | bytes 2621440 | tf_op jit(solution)/shard_map/all_gather | solution.py:86
Sparse Core Ops, SparseCore 0:
  10.8 63.1 all-gather.7
  76.8 74.3 all-gather.5
  153.5 96.0 reduce-scatter.4
  252.2 78.3 reduce-scatter.2
  333.9 58.0 all-gather.9
  416.6 31.1 all-gather.11
  449.9 44.5 all-gather.13
where the time goes:
time: 506 us; the launch traced here: 505 us
  waiting for transfers between devices  365 us (72%)
  blocking collectives  81 us (16%)
  matrix products  27.1 us (5%)
  between operations  15.7 us (3%)
  local copies, waits for them, and re-layouts  12 us (2%)
    reduce_scatter x1, waiting for transfers between devices, body(): lax.psum_scatter(split_rows(output_inner, layer_cotangent), ('rep', 'fs')...  87.6 us
    reduce_scatter x1, waiting for transfers between devices, body(): lax.psum_scatter(split_rows(query_inner, query_cotangent), ('rep', 'fs'),...  79.1 us
    all_gather x1, waiting for transfers between devices, body(): lax.all_gather(output_basis, ('rep', 'fs'), axis=0, tiled=True)  65.3 us
    all_gather x1, waiting for transfers between devices, body(): lax.all_gather(query_basis, ('rep', 'fs'), axis=0, tiled=True)  65 us
    all_gather x1, blocking collectives, body(): lax.all_gather(normed_q.astype(jnp.bfloat16), ('rep', 'fs'), axis=0, tile...  43.2 us
    all_gather x1, waiting for transfers between devices, body(): lax.all_gather((output_weight - step_rate * update_o).astype(jnp.bfloat16...  43.1 us
    psum x1, blocking collectives, body(): lax.psum((jnp.sum(normed_q * normed_q), jnp.sum(normed_o * normed_o)), ('...  37.8 us
    all_gather x1, waiting for transfers between devices, body(): lax.all_gather((query_weight - step_rate * update_q).astype(jnp.bfloat16)...  23.8 us
  transfers between devices with their start and end apart: 7, of which 6 were waited for; matrix products, arithmetic and copies ran while one was open for 8% of the time, Pallas kernels for 0%

commit v1 on v0

v1 whole, which is shorter than its diff:
```python
import functools

import jax
import jax.numpy as jnp
from jax import lax
from jax.experimental import pallas as pl
from jax.experimental.pallas import tpu as pltpu
from jax.sharding import PartitionSpec as P

MESH = pl.DeviceIdType.MESH
DMA = pltpu.SemaphoreType.DMA

beta_first = 0.6
beta_second = 0.8
step_rate = 0.01
small_eps = 1e-06


def here():
    return lax.axis_index("fs"), lax.axis_index("rep"), lax.axis_index("tp")


def flip(rep, bit):
    if bit == 1:
        return rep + 1 - 2 * lax.rem(rep, 2)
    return lax.rem(rep + 2, 4)


def remote(src, dst, send, recv, device):
    return pltpu.make_async_remote_copy(
        src_ref=src, dst_ref=dst, send_sem=send, recv_sem=recv, device_id=device, device_id_type=MESH
    )


def greet(devices):
    barrier = pltpu.get_barrier_semaphore()
    count = 0
    for device, present in devices:
        if present is True:
            pl.semaphore_signal(barrier, inc=1, device_id=device, device_id_type=MESH)
            count = count + 1
        else:
            count = count + present.astype(jnp.int32)

            @pl.when(present)
            def _():
                pl.semaphore_signal(barrier, inc=1, device_id=device, device_id_type=MESH)

    pl.semaphore_wait(barrier, count)


class Line:
    def __init__(self, n, view, send, recv):
        self.n, self.view, self.send_sem, self.recv_sem = n, view, send, recv
        self.fs, self.rep, self.tp = here()

    def outgoing(self, step, way):
        fs, n = self.fs, self.n
        if way == 0:
            block, peer = fs - step + 1, fs + 1
            present = jnp.logical_and(block >= 0, peer < n)
        else:
            block, peer = fs + step - 1, fs - 1
            present = jnp.logical_and(block < n, peer >= 0)
        block = lax.rem(block + n, n)
        peer = lax.rem(peer + n, n)
        view = self.view(block)
        sems = (self.send_sem.at[way, step - 1], self.recv_sem.at[way, step - 1])
        return remote(view, view, *sems, (peer, self.rep, self.tp)), present

    def incoming(self, step, way):
        fs, n = self.fs, self.n
        block = fs - step if way == 0 else fs + step
        present = block >= 0 if way == 0 else block < n
        block = lax.rem(block + n, n)
        view = self.view(block)
        sems = (self.send_sem.at[way, step - 1], self.recv_sem.at[way, step - 1])
        return remote(view, view, *sems, (fs, self.rep, self.tp)), present, block

    def start(self, step):
        for way in (0, 1):
            copy, present = self.outgoing(step, way)

            @pl.when(present)
            def _():
                copy.start()

    def arrive(self, step):
        for way in (0, 1):
            copy, present, _ = self.incoming(step, way)

            @pl.when(present)
            def _():
                copy.wait_recv()

    def sent(self):
        for step in range(1, self.n):
            for way in (0, 1):
                copy, present = self.outgoing(step, way)

                @pl.when(present)
                def _():
                    copy.wait_send()


def gather(n, views, line_sems, one_sems, two_sems, third_sems=None, between=None):
    fs, rep, tp = here()
    lines = [
        Line(n, lambda b, v=v: v(rep * n + b, None), line_sems[0].at[a], line_sems[1].at[a])
        for a, v in enumerate(views)
    ]
    bits = ((1, 2), (2, 1))

    def slots():
        yield 0, 0, 0
        for step in range(1, n):
            yield step, 0, 2 * step - 1
            yield step, 1, 2 * step

    def block_of(step, way):
        if step == 0:
            return fs, True
        block = fs - step if way == 0 else fs + step
        present = block >= 0 if way == 0 else block < n
        return lax.rem(block + n, n), present

    def when(present, body):
        if present is True:
            body()
        else:
            pl.when(present)(body)

    def one(a, block, slot, half):
        peer = flip(rep, bits[half][0])
        view = views[a](rep * n + block, half)
        return remote(view, view, one_sems[0].at[a, half, slot], one_sems[1].at[a, half, slot], (fs, peer, tp))

    def one_in(a, block, slot, half):
        peer = flip(rep, bits[half][0])
        view = views[a](peer * n + block, half)
        return remote(view, view, one_sems[0].at[a, half, slot], one_sems[1].at[a, half, slot], (fs, peer, tp))

    def two(a, block, slot, half, which):
        peer = flip(rep, bits[half][1])
        held = rep if which == 0 else flip(rep, bits[half][0])
        view = views[a](held * n + block, half)
        sems = [s.at[a, half, which, slot] for s in two_sems]
        return remote(view, view, *sems, (fs, peer, tp))

    def two_in(a, block, slot, half, which):
        peer = flip(rep, bits[half][1])
        held = peer if which == 0 else flip(peer, bits[half][0])
        view = views[a](held * n + block, half)
        sems = [s.at[a, half, which, slot] for s in two_sems]
        return remote(view, view, *sems, (fs, peer, tp))

    def third(a, block, group):
        view = views[a](group * n + block, None)
        sems = [s.at[a, group, block] for s in third_sems]
        return remote(view, view, *sems, (fs, rep, 1 - tp))

    def third_in(a, block, group):
        view = views[a](group * n + block, None, 1 - tp)
        sems = [s.at[a, group, block] for s in third_sems]
        return remote(view, view, *sems, (fs, rep, 1 - tp))

    arrays = range(len(views))

    def launch(step, way, slot):
        block, present = block_of(step, way)

        def body():
            for a in arrays:
                for half in (0, 1):
                    one(a, block, slot, half).start()
                for half in (0, 1):
                    two(a, block, slot, half, 0).start()

        when(present, body)

    def relay(step, way, slot):
        block, present = block_of(step, way)

        def body():
            for a in arrays:
                for half in (0, 1):
                    one_in(a, block, slot, half).wait_recv()
                    two(a, block, slot, half, 1).start()

        when(present, body)

    def finish(step, way, slot):
        block, present = block_of(step, way)

        def body():
            for a in arrays:
                for half in (0, 1):
                    for which in (0, 1):
                        two_in(a, block, slot, half, which).wait_recv()
                if third_sems is not None:
                    for group in range(4):
                        third(a, block, group).start()

        when(present, body)

    def drain(step, way, slot):
        block, present = block_of(step, way)

        def body():
            for a in arrays:
                for half in (0, 1):
                    one(a, block, slot, half).wait_send()
                    for which in (0, 1):
                        two(a, block, slot, half, which).wait_send()
                if third_sems is not None:
                    for group in range(4):
                        third(a, block, group).wait_send()
                        third_in(a, block, group).wait_recv()

        when(present, body)

    order = list(slots())
    for step in range(n):
        if step:
            for line in lines:
                line.arrive(step)
        if step < n - 1:
            for line in lines:
                line.start(step + 1)
        if step == 0 and between is not None:
            between()
        for s, way, slot in order:
            if s == step:
                launch(s, way, slot)
        for s, way, slot in order:
            if s == step - 1:
                relay(s, way, slot)
    for s, way, slot in order:
        if s == n - 1:
            relay(s, way, slot)
    for s, way, slot in order:
        finish(s, way, slot)
    for s, way, slot in order:
        drain(s, way, slot)
    for line in lines:
        line.sent()


def pairs(*shapes):
    return [DMA(shape) for shape in shapes for _ in (0, 1)]


def first_kernel(
    n, bq_ref, bo_ref, w_ref, gq_ref, go_ref, gw_ref,
    local, ls, lr, os, orr, ts, tr, hs, hr, ws, wr,
):
    fs, rep, tp = here()
    mine = rep * n + fs
    copies = [
        pltpu.make_async_copy(bq_ref, gq_ref.at[mine], local.at[0]),
        pltpu.make_async_copy(bo_ref, go_ref.at[mine], local.at[1]),
        pltpu.make_async_copy(w_ref, gw_ref.at[fs], local.at[2]),
    ]
    for copy in copies:
        copy.start()
    peers = [((lax.rem(fs + 1, n), rep, tp), fs + 1 < n), ((lax.rem(fs + n - 1, n), rep, tp), fs >= 1)]
    peers += [((fs, flip(rep, bit), tp), True) for bit in (1, 2)]
    peers += [((fs, rep, 1 - tp), True)]
    for copy in copies:
        copy.wait()
    greet(peers)

    def view_of(ref):
        rows, cols = ref.shape[1] // 2, ref.shape[2] // 2

        def view(block, half, core=None):
            core = tp if core is None else core
            span = pl.ds(pl.multiple_of(core * cols, cols), cols)
            if half is None:
                return ref.at[block, :, span]
            return ref.at[block, pl.ds(half * rows, rows), span]

        return view

    weights = Line(n, lambda b: gw_ref.at[b], ws, wr)
    gather(
        n, [view_of(gq_ref), view_of(go_ref)], (ls, lr), (os, orr), (ts, tr), (hs, hr),
        between=lambda: weights.start(1),
    )
    for step in range(1, n):
        weights.arrive(step)
        if step < n - 1:
            weights.start(step + 1)
    weights.sent()


def gather_bases(n, basis_q, basis_o, weight):
    slots = 2 * n - 1
    whole = lambda a: jax.ShapeDtypeStruct((4 * n, *a.shape), a.dtype)
    vmem = pl.BlockSpec(memory_space=pltpu.VMEM)
    return pl.pallas_call(
        functools.partial(first_kernel, n),
        out_shape=(whole(basis_q), whole(basis_o), jax.ShapeDtypeStruct((n, *weight.shape), weight.dtype)),
        in_specs=[vmem] * 3,
        out_specs=(vmem,) * 3,
        scratch_shapes=[DMA((3,))]
        + pairs((2, 2, n - 1), (2, 2, slots), (2, 2, 2, slots), (2, 4, n), (2, n - 1)),
        compiler_params=pltpu.CompilerParams(
            collective_id=0, has_side_effects=True, vmem_limit_bytes=40 * 2**20
        ),
        name="gather_bases",
    )(basis_q, basis_o, weight)


def second_kernel(
    n, pq_ref, po_ref, fq_ref, sq_ref, fo_ref, so_ref, w_ref,
    nfq_ref, nsq_ref, nfo_ref, nso_ref, gq_ref, go_ref, gw_ref, tot_ref,
    rq, ro, aq, ao, zq, zo, gs, local,
    rs, rr, zs, zr, ls, lr, os, orr, ts, tr, ws, wr, cs, cr,
):
    fs, rep, tp = here()
    mine = rep * n + fs
    own = pltpu.make_async_copy(w_ref, gw_ref.at[fs], local.at[0])
    own.start()
    peers = [((lax.rem(fs + k, n), rep, tp), True) for k in range(1, n)]
    peers += [((fs, lax.rem(rep + k, 4), tp), True) for k in range(1, 4)]
    peers += [((fs, rep, 1 - tp), True)]
    own.wait()
    greet(peers)
    weights = Line(n, lambda b: gw_ref.at[b], ws, wr)

    parts, heard, summed, late = (pq_ref, po_ref), (rq, ro), (aq, ao), (zq, zo)

    def swap(a, j, k):
        f, to = lax.rem(fs + j, n), lax.rem(rep + k, 4)
        sems = (rs.at[a, j - 1, k - 1], rr.at[a, j - 1, k - 1])
        return remote(parts[a].at[to * n + f], heard[a].at[j - 1, k - 1], *sems, (fs, to, tp))

    def cross(a, j):
        f = lax.rem(fs + j, n)
        return remote(
            summed[a].at[j - 1], late[a].at[j - 1], zs.at[a, j - 1], zr.at[a, j - 1], (f, rep, tp)
        )

    for j in range(1, n + 1):
        for a in (1, 0):
            for k in (2, 1, 3):
                swap(a, j, k).start()
    weights.start(1)
    final = [None, None]
    for j in range(1, n + 1):
        f = lax.rem(fs + j, n)
        for a in (1, 0):
            for k in (2, 1, 3):
                swap(a, j, k).wait_recv()
            total = parts[a][rep * n + f].astype(jnp.float32)
            for k in (1, 2, 3):
                total = total + heard[a][j - 1, k - 1].astype(jnp.float32)
            if j < n:
                summed[a][j - 1] = total.astype(jnp.bfloat16)
                cross(a, j).start()
            else:
                final[a] = total
    for a in (0, 1):
        for j in range(1, n):
            cross(a, j).wait_recv()
        for j in range(1, n):
            final[a] = final[a] + late[a][j - 1].astype(jnp.float32)
    refs = ((fq_ref, sq_ref, nfq_ref, nsq_ref, gq_ref), (fo_ref, so_ref, nfo_ref, nso_ref, go_ref))
    for a in (0, 1):
        first, second, first_out, second_out, g = refs[a]
        first_next = beta_first * first[...] + (1.0 - beta_first) * final[a]
        second_next = beta_second * second[...] + (1.0 - beta_second) * final[a] * final[a]
        normed = first_next / jnp.sqrt(second_next)
        first_out[...] = first_next
        second_out[...] = second_next
        g[mine] = normed.astype(jnp.bfloat16)
        square = normed * normed
        rows, cols = square.shape
        square = sum(square[:, c : c + 128] for c in range(0, cols, 128))
        square = sum(square[r : r + 8] for r in range(0, rows, 8))
        gs[mine, :, a * 128 : (a + 1) * 128] = square

    def view_of(ref):
        cols = ref.shape[2] // 2

        def view(block, half):
            if half is None:
                return ref.at[block]
            return ref.at[block, :, pl.ds(half * cols, cols)]

        return view

    gather(n, [view_of(go_ref), view_of(gq_ref), view_of(gs)], (ls, lr), (os, orr), (ts, tr))
    for step in range(1, n):
        weights.arrive(step)
        if step < n - 1:
            weights.start(step + 1)
    tot_ref[0] = sum(gs[b] for b in range(4 * n))
    pair = remote(tot_ref.at[0], tot_ref.at[1], cs.at[0], cr.at[0], (fs, rep, 1 - tp))
    pair.start()
    pair.wait()
    weights.sent()
    for j in range(1, n + 1):
        for a in (0, 1):
            for k in (1, 2, 3):
                swap(a, j, k).wait_send()
            if j < n:
                cross(a, j).wait_send()


def advance(n, part_q, part_o, first_q, second_q, first_o, second_o, weight):
    slots = 2 * n - 1
    rows, cq = first_q.shape
    co = first_o.shape[1]
    f32, b16 = jnp.float32, jnp.bfloat16
    shape = jax.ShapeDtypeStruct
    vmem = pl.BlockSpec(memory_space=pltpu.VMEM)
    return pl.pallas_call(
        functools.partial(second_kernel, n),
        out_shape=(
            shape((rows, cq), f32), shape((rows, cq), f32), shape((rows, co), f32), shape((rows, co), f32),
            shape((4 * n, rows, cq), b16), shape((4 * n, rows, co), b16),
            shape((n, *weight.shape), b16), shape((2, 8, 256), f32),
        ),
        in_specs=[vmem] * 7,
        out_specs=(vmem,) * 8,
        scratch_shapes=[
            pltpu.VMEM((n, 3, rows, cq), b16), pltpu.VMEM((n, 3, rows, co), b16),
            pltpu.VMEM((n - 1, rows, cq), b16), pltpu.VMEM((n - 1, rows, co), b16),
            pltpu.VMEM((n - 1, rows, cq), b16), pltpu.VMEM((n - 1, rows, co), b16),
            pltpu.VMEM((4 * n, 8, 256), f32), DMA((1,)),
        ]
        + pairs((2, n, 3), (2, n - 1), (3, 2, n - 1), (3, 2, slots), (3, 2, 2, slots), (2, n - 1), (1,)),
        compiler_params=pltpu.CompilerParams(
            collective_id=1, has_side_effects=True, vmem_limit_bytes=48 * 2**20
        ),
        name="advance",
    )(part_q, part_o, first_q, second_q, first_o, second_o, weight)


def body(
    n,
    query_input,
    query_cotangent,
    branch_output,
    layer_cotangent,
    query_weight,
    output_weight,
    query_basis,
    output_basis,
    query_first,
    query_second,
    output_first,
    output_second,
):
    f32, b16 = jnp.float32, jnp.bfloat16
    rank = query_basis.shape[1]
    gq, go, wq = gather_bases(n, query_basis, output_basis, query_weight.astype(b16))
    whole_q, whole_o = gq.reshape(-1, rank), go.reshape(-1, rank)

    def project(inputs, basis, cotangent):
        inner = jnp.dot(inputs, basis, preferred_element_type=f32).astype(b16)
        part = lax.dot_general(inner, cotangent, (((0,), (0,)), ((), ())), preferred_element_type=f32)
        return part.astype(b16).reshape(4 * n, -1, cotangent.shape[1])

    part_q = project(query_input, whole_q, query_cotangent)
    part_o = project(branch_output, whole_o, layer_cotangent)
    first_q, second_q, first_o, second_o, nq, no, wo, totals = advance(
        n, part_q, part_o, query_first, query_second, output_first, output_second, output_weight.astype(b16)
    )
    sums = jnp.sum(totals.reshape(16, 2, 128), axis=(0, 2))
    rep = lax.axis_index("rep")

    def update(basis, whole, normed, total, weights):
        normed = normed.reshape(rank, -1)
        columns = normed.shape[1]
        scale = lax.rsqrt(total / (rank * 2 * columns) + small_eps)
        mine = scale * jnp.dot(basis, normed, preferred_element_type=f32)
        weights = weights.reshape(-1, columns)
        count = weights.shape[0]
        rows = lax.dynamic_slice_in_dim(whole, rep * count, count)
        group = scale * jnp.dot(rows, normed, preferred_element_type=f32)
        return mine, (weights.astype(f32) - step_rate * group).astype(b16)

    update_q, copy_q = update(query_basis, whole_q, nq, sums[0], wq)
    update_o, copy_o = update(output_basis, whole_o, no, sums[1], wo)
    return (update_q, update_o, first_q, second_q, first_o, second_o, copy_q, copy_o)


def solution(mesh):
    in_specs = (
        P(("fs", "rep"), None),
        P(("fs", "rep"), "tp"),
        P(("fs", "rep"), None),
        P(("fs", "rep"), "tp"),
        P(("rep", "fs"), "tp"),
        P(("rep", "fs"), "tp"),
        P(("rep", "fs"), None),
        P(("rep", "fs"), None),
        P(("rep", "fs"), "tp"),
        P(("rep", "fs"), "tp"),
        P(("rep", "fs"), "tp"),
        P(("rep", "fs"), "tp"),
    )
    out_specs = (
        P(("rep", "fs"), "tp"),
        P(("rep", "fs"), "tp"),
        P(("rep", "fs"), "tp"),
        P(("rep", "fs"), "tp"),
        P(("rep", "fs"), "tp"),
        P(("rep", "fs"), "tp"),
        P("rep", "tp"),
        P("rep", "tp"),
    )
    n = mesh.shape["fs"]
    assert mesh.shape["rep"] == 4 and mesh.shape["tp"] == 2
    return jax.shard_map(functools.partial(body, n), mesh=mesh, in_specs=in_specs, out_specs=out_specs, check_vma=False)
```

time: 506 us -> 189 us (0.37)
  waiting for transfers between devices: 365 us -> 0 us
  Pallas kernels: 0 us -> 136 us
  blocking collectives: 81 us -> 0 us
  between operations: 15.7 us -> 2.22 us
  local copies, waits for them, and re-layouts: 12 us -> 17.1 us
    all_gather x5 -> x0, waiting for transfers between devices: 197 us -> none  [the longest x1 65.3 us: body(): lax.all_gather(output_basis, ('rep', 'fs'), axis=0, tiled=True)]
    reduce_scatter x2 -> x0, waiting for transfers between devices: 167 us -> none  [the longest x1 87.6 us: body(): lax.psum_scatter(split_rows(output_inner, layer_cotangent), ('rep', 'fs')...]
    pallas_call x0 -> x2, Pallas kernels: none -> 136 us  [the longest x1 83.8 us: advance(): pl.pallas_call(functools.partial(second_kernel, n), out_shape=(shape((row...]
    all_gather x1 -> x0, blocking collectives: 43.2 us -> none  [body(): lax.all_gather(normed_q.astype(jnp.bfloat16), ('rep', 'fs'), axis=0, tile...]
    psum x1 -> x0, blocking collectives: 37.8 us -> none  [body(): lax.psum((jnp.sum(normed_q * normed_q), jnp.sum(normed_o * normed_o)), ('...]
    dot_general x8 -> x6, matrix products: 27.1 us -> 31.7 us  [the longest x2 20.7 us: project(): lax.dot_general(inner, cotangent, (((0,), (0,)), ((), ())), preferred_ele...]
    unnamed x32 -> x52, local copies, waits for them, and re-layouts: 12 us -> 16.5 us
  transfers between devices with their start and end apart: 7 -> 0, of which waited for: 6 -> 0; matrix products, arithmetic and copies ran while one was open for 8% -> 0% of each run, Pallas kernels for 0% -> 0%
where the time goes in v1:
time: 189 us; the launch traced here: 188 us
  Pallas kernels  136 us (72%)
  matrix products  31.7 us (17%)
  local copies, waits for them, and re-layouts  17.1 us (9%)
  between operations  2.22 us (1%)
    pallas_call x1, Pallas kernels, advance(): pl.pallas_call(functools.partial(second_kernel, n), out_shape=(shape((row...  83.8 us
    pallas_call x1, Pallas kernels, gather_bases(): pl.pallas_call(functools.partial(first_kernel, n), out_shape=(whole(basis...  52.1 us
    dot_general x2, matrix products, project(): lax.dot_general(inner, cotangent, (((0,), (0,)), ((), ())), preferred_ele...  20.7 us
    unnamed x52, local copies, waits for them, and re-layouts  16.5 us
    dot_general x2, matrix products, update(): group = scale * jnp.dot(rows, normed, preferred_element_type=f32)  7.86 us

profile of v1, /device:TPU:0, one launch (start us, length us, event | category | flops | bytes accessed | tf_op | source)
XLA Modules:
  0.0 188.3 jit_solution(12356376428139595547)
XLA Ops:
  0.6 0.0 copy-start
  0.6 1.2 convert_element_type.38.w_ref
  1.8 0.0 copy-start.1
  1.8 0.9 copy-done.1
  2.8 0.0 copy-start.4
  2.8 0.9 copy-done.4
  3.7 52.1 %gather_bases.1 = (bf16[16,256,512]{2,1,0:T(8,128)(2,1)S(1)}, bf16[16,128,512]{2,1,0:T(8,128)(2,1)S(1)}, bf16[4,256,512]{2,1,0:T(8,128)(2,1)S(1)}) custom-call(bf16[256,512]{1,0:T(8,128)(2,1)S(1)} %copy-done.1, bf16[128,512]{1,0:T(8,128)(2,1)S(1)} %copy-done.4, bf16[256,512]{1,0:T(8,128)(2,1)S(1)} %convert_element_type.38.w_ref), custom_call_target="tpu_custom_call" | custom-call | tf_op jit(solution)/shard_map/gather_bases/pallas_call | solution.py:301
  55.8 0.0 copy-start.19
  55.8 1.9 %copy-done.19 = bf16[16,256,512]{2,1,0:T(8,128)(2,1)} copy-done((bf16[16,256,512]{2,1,0:T(8,128)(2,1)}, bf16[16,256,512]{2,1,0:T(8,128)(2,1)S(1)}, u32[]{:S(2)}) %copy-start.19) | copy-done | bytes 4194328
  57.8 0.0 copy-start.21
  57.8 1.0 copy-done.21
  58.7 0.0 copy-start.20
  58.7 10.1 %convolution_convert_fusion = bf16[512,2048]{1,0:T(8,128)(2,1)} fusion(bf16[1024,2048]{1,0:T(8,128)(2,1)} %param.15, bf16[2048,512]{1,0:T(8,128)(2,1)S(1)} %bitcast.37, bf16[1024,2048]{1,0:T(8,128)(2,1)} %param.14), kind=kOutput, calls=%fused_computation.2 | convolution fusion | flops 4296540160 | bytes 12582912 | tf_op jit(solution)/shard_map/dot_general | solution.py:464
  68.8 0.0 copy-done.20
  68.8 0.0 copy-done
  68.8 0.0 copy-start.22
  68.8 0.0 copy-start.11
  68.8 0.0 copy-start.17
  68.8 0.0 copy-start.18
  68.9 10.6 %convolution_convert_fusion.3 = bf16[512,512]{1,0:T(8,128)(2,1)} fusion(bf16[1024,512]{1,0:T(8,128)(2,1)S(1)} %copy-done, bf16[4096,512]{1,0:T(8,128)(2,1)} %bitcast.35, bf16[1024,4096]{1,0:T(8,128)(2,1)} %param.12), kind=kOutput, calls=%fused_computation.9 | convolution fusion | flops 4832624640 | bytes 14155776 | tf_op jit(solution)/shard_map/dot_general | solution.py:464
  79.5 0.0 copy-done.22
  79.5 0.1 convert_element_type.43.w_ref
  79.6 0.0 copy-done.11
  79.6 0.0 copy-done.17
  79.6 0.0 copy-done.18
  79.6 0.0 copy-start.6
  79.6 1.0 copy-done.6
  80.6 0.0 copy-start.12
  80.6 0.9 copy-done.12
  81.6 83.8 %advance.1 = (f32[32,512]{1,0:T(8,128)S(1)}, f32[32,512]{1,0:T(8,128)S(1)}, f32[32,2048]{1,0:T(8,128)S(1)}, f32[32,2048]{1,0:T(8,128)S(1)}, bf16[16,32,512]{2,1,...) custom-call(bf16[16,32,512]{2,1,0:T(8,128)(2,1)S(1)} %bitcast.34, ...), custom_call_target="tpu_custom_call" | custom-call | tf_op jit(solution)/shard_map/advance/pallas_call | solution.py:419
  165.4 0.0 copy-start.3
  165.4 0.8 copy-done.3
  166.2 0.0 copy-start.7
  166.2 0.7 copy-done.7
  166.9 0.0 copy-start.9
  166.9 0.7 copy-done.9
  167.6 0.0 copy-start.13
  167.6 0.6 copy-done.13
  168.2 0.0 copy-start.15
  168.2 0.6 copy-done.15
  168.9 0.1 bitcast_reduce_fusion
  169.0 0.6 fusion.8
  170.3 4.4 %fusion = bf16[512,2048]{1,0:T(8,128)(2,1)} fusion(bf16[512,2048]{1,0:T(8,128)(2,1)} %bitcast.41, bf16[512,2048]{1,0:T(8,128)(2,1)S(1)} %bitcast.30, f32[]{:T(128)} %bitcast.8, bf16[2048,512]{1,0:T(8,128)(2,1)} %bitcast.38, s32[]{:T(128)S(6)} %select_n.7), kind=kOutput, calls=%fused_computation.1 | convolution fusion | flops 1078984704 | bytes 6816260 | tf_op jit(solution)/shard_map/dot_general | solution.py:483
  174.7 0.0 copy-start.5
  175.5 3.4 %fusion.2 = bf16[1024,512]{1,0:T(8,128)(2,1)} fusion(bf16[1024,512]{1,0:T(8,128)(2,1)} %bitcast.39, bf16[512,512]{1,0:T(8,128)(2,1)} %bitcast.32, bf16[4096,512]{1,0:T(8,128)(2,1)} %bitcast.36, s32[]{:T(128)S(6)} %select_n.6, f32[]{:T(128)} %bitcast.5), kind=kOutput, calls=%fused_computation.6 | convolution fusion | flops 539492352 | bytes 3670532 | tf_op jit(solution)/shard_map/dot_general | solution.py:483
  178.9 0.0 copy-done.5
  178.9 0.0 copy-start.2
  178.9 1.7 fusion.1
  180.6 0.0 copy-start.16
  180.6 0.0 copy-start.14
  180.6 0.0 copy-start.10
  180.6 0.0 copy-start.8
  180.6 2.6 %copy.23 = f32[128,2048]{1,0:T(8,128)} copy(f32[128,2048]{0,1:T(8,128)} %fusion.1) | data formatting | bytes 2097152
  183.2 0.0 copy-done.2
  183.2 1.4 fusion.3
  184.6 1.0 copy.22
  185.6 0.0 copy-done.16
  185.6 0.6 copy.28
  186.3 0.0 copy-done.14
  186.3 0.6 copy.29
  186.9 0.0 copy-done.10
  186.9 0.7 copy.30
  187.6 0.0 copy-done.8
  187.6 0.7 copy.31
  (1 shorter events, 0.0 us)
Async XLA Ops:
  0.6 68.2 %copy-start = (bf16[1024,512]{1,0:T(8,128)(2,1)S(1)}, bf16[1024,512]{1,0:T(8,128)(2,1)}, u32[]{:S(2)}) copy-start(bf16[1024,512]{1,0:T(8,128)(2,1)} %param.13) | copy-start | bytes 3145732
  1.8 1.0 copy-start.1
  2.8 0.9 copy-start.4
  55.8 1.9 %copy-start.19 = (bf16[16,256,512]{2,1,0:T(8,128)(2,1)}, bf16[16,256,512]{2,1,0:T(8,128)(2,1)S(1)}, u32[]{:S(2)}) copy-start(bf16[16,256,512]{2,1,0:T(8,128)(2,1)S(1)} %get-tuple-element.19) | copy-start | bytes 12582916
  57.8 1.0 copy-start.21
  58.7 10.1 %copy-start.20 = (bf16[16,128,512]{2,1,0:T(8,128)(2,1)}, bf16[16,128,512]{2,1,0:T(8,128)(2,1)S(1)}, u32[]{:S(2)}) copy-start(bf16[16,128,512]{2,1,0:T(8,128)(2,1)S(1)} %get-tuple-element.20) | copy-start | bytes 6291460
  68.8 10.7 %copy-start.22 = (f32[128,2048]{1,0:T(8,128)S(1)}, f32[128,2048]{1,0:T(8,128)}, u32[]{:S(2)}) copy-start(f32[128,2048]{1,0:T(8,128)} %param.17) | copy-start | bytes 3145732
  68.8 10.7 %copy-start.11 = (f32[32,2048]{1,0:T(8,128)S(1)}, f32[32,2048]{1,0:T(8,128)}, u32[]{:S(2)}) copy-start(f32[32,2048]{1,0:T(8,128)} %fo_ref.1) | copy-start | bytes 786436
  68.8 10.7 %copy-start.17 = (f32[32,512]{1,0:T(8,128)S(1)}, f32[32,512]{1,0:T(8,128)}, u32[]{:S(2)}) copy-start(f32[32,512]{1,0:T(8,128)} %fq_ref.1) | copy-start | bytes 196612
  68.8 10.7 %copy-start.18 = (f32[32,512]{1,0:T(8,128)S(1)}, f32[32,512]{1,0:T(8,128)}, u32[]{:S(2)}) copy-start(f32[32,512]{1,0:T(8,128)} %sq_ref.1) | copy-start | bytes 196612
  79.6 1.0 copy-start.6
  80.6 0.9 copy-start.12
  165.4 0.8 copy-start.3
  166.2 0.7 copy-start.7
  166.9 0.7 copy-start.9
  167.6 0.6 copy-start.13
  168.2 0.6 copy-start.15
  174.7 4.2 %copy-start.5 = (bf16[128,512]{1,0:T(8,128)(2,1)S(1)}, bf16[128,512]{1,0:T(8,128)(2,1)}, u32[]{:S(2)}) copy-start(bf16[128,512]{1,0:T(8,128)(2,1)} %bo_ref.1) | copy-start | bytes 393220
  178.9 4.3 %copy-start.2 = (bf16[256,512]{1,0:T(8,128)(2,1)S(1)}, bf16[256,512]{1,0:T(8,128)(2,1)}, u32[]{:S(2)}) copy-start(bf16[256,512]{1,0:T(8,128)(2,1)} %bq_ref.1) | copy-start | bytes 786436
  180.6 5.0 %copy-start.16 = (f32[32,512]{1,0:T(8,128)S(1)}, f32[32,512]{1,0:T(8,128)}, u32[]{:S(2)}) copy-start(f32[32,512]{1,0:T(8,128)} %copy-done.15) | copy-start | bytes 196612
  180.6 5.6 %copy-start.14 = (f32[32,512]{1,0:T(8,128)S(1)}, f32[32,512]{1,0:T(8,128)}, u32[]{:S(2)}) copy-start(f32[32,512]{1,0:T(8,128)} %copy-done.13) | copy-start | bytes 196612
  180.6 6.3 %copy-start.10 = (f32[32,2048]{1,0:T(8,128)S(1)}, f32[32,2048]{1,0:T(8,128)}, u32[]{:S(2)}) copy-start(f32[32,2048]{1,0:T(8,128)} %copy-done.9) | copy-start | bytes 786436
  180.6 7.0 %copy-start.8 = (f32[32,2048]{1,0:T(8,128)S(1)}, f32[32,2048]{1,0:T(8,128)}, u32[]{:S(2)}) copy-start(f32[32,2048]{1,0:T(8,128)} %copy-done.7) | copy-start | bytes 786436

commit v2 on v1

--- a/solution.py
+++ b/solution.py
@@ -53,6 +53,14 @@
     def __init__(self, n, view, send, recv):
         self.n, self.view, self.send_sem, self.recv_sem = n, view, send, recv
         self.fs, self.rep, self.tp = here()
+        self.done = 0
+
+    def tick(self):
+        if 0 < self.done < self.n:
+            self.arrive(self.done)
+        if self.done + 1 < self.n:
+            self.start(self.done + 1)
+        self.done += 1
 
     def outgoing(self, step, way):
         fs, n = self.fs, self.n
@@ -103,7 +111,7 @@
                     copy.wait_send()
 
 
-def gather(n, views, line_sems, one_sems, two_sems, third_sems=None, between=None):
+def gather(n, views, line_sems, one_sems, two_sems, third_sems=None, ticks=()):
     fs, rep, tp = here()
     lines = [
         Line(n, lambda b, v=v: v(rep * n + b, None), line_sems[0].at[a], line_sems[1].at[a])
@@ -227,19 +235,32 @@
         if step < n - 1:
             for line in lines:
                 line.start(step + 1)
-        if step == 0 and between is not None:
-            between()
+        if step == n - 2:
+            for side in ticks:
+                side.tick()
         for s, way, slot in order:
             if s == step:
                 launch(s, way, slot)
         for s, way, slot in order:
             if s == step - 1:
                 relay(s, way, slot)
+            if s == step - 2:
+                finish(s, way, slot)
+    for side in ticks:
+        side.tick()
     for s, way, slot in order:
         if s == n - 1:
             relay(s, way, slot)
+        if s == n - 2:
+            finish(s, way, slot)
+    for side in ticks:
+        side.tick()
     for s, way, slot in order:
-        finish(s, way, slot)
+        if s == n - 1:
+            finish(s, way, slot)
+    for side in ticks:
+        while side.done < n:
+            side.tick()
     for s, way, slot in order:
         drain(s, way, slot)
     for line in lines:
@@ -251,7 +272,7 @@
 
 
 def first_kernel(
-    n, bq_ref, bo_ref, w_ref, gq_ref, go_ref, gw_ref,
+    n, bq_ref, bo_ref, w_ref, v_ref, gq_ref, go_ref, gw_ref, gv_ref,
     local, ls, lr, os, orr, ts, tr, hs, hr, ws, wr,
 ):
     fs, rep, tp = here()
@@ -260,6 +281,7 @@
         pltpu.make_async_copy(bq_ref, gq_ref.at[mine], local.at[0]),
         pltpu.make_async_copy(bo_ref, go_ref.at[mine], local.at[1]),
         pltpu.make_async_copy(w_ref, gw_ref.at[fs], local.at[2]),
+        pltpu.make_async_copy(v_ref, gv_ref.at[fs], local.at[3]),
     ]
     for copy in copies:
         copy.start()
@@ -282,34 +304,33 @@
 
         return view
 
-    weights = Line(n, lambda b: gw_ref.at[b], ws, wr)
+    weights = [
+        Line(n, lambda b, g=g: g.at[b], ws.at[i], wr.at[i]) for i, g in enumerate((gw_ref, gv_ref))
+    ]
     gather(
-        n, [view_of(gq_ref), view_of(go_ref)], (ls, lr), (os, orr), (ts, tr), (hs, hr),
-        between=lambda: weights.start(1),
+        n, [view_of(gq_ref), view_of(go_ref)], (ls, lr), (os, orr), (ts, tr), (hs, hr), ticks=weights
     )
-    for step in range(1, n):
-        weights.arrive(step)
-        if step < n - 1:
-            weights.start(step + 1)
-    weights.sent()
-
-
-def gather_bases(n, basis_q, basis_o, weight):
+    for side in weights:
+        side.sent()
+
+
+def gather_bases(n, basis_q, basis_o, *weights):
     slots = 2 * n - 1
     whole = lambda a: jax.ShapeDtypeStruct((4 * n, *a.shape), a.dtype)
     vmem = pl.BlockSpec(memory_space=pltpu.VMEM)
     return pl.pallas_call(
         functools.partial(first_kernel, n),
-        out_shape=(whole(basis_q), whole(basis_o), jax.ShapeDtypeStruct((n, *weight.shape), weight.dtype)),
-        in_specs=[vmem] * 3,
-        out_specs=(vmem,) * 3,
-        scratch_shapes=[DMA((3,))]
-        + pairs((2, 2, n - 1), (2, 2, slots), (2, 2, 2, slots), (2, 4, n), (2, n - 1)),
+        out_shape=(whole(basis_q), whole(basis_o))
+        + tuple(jax.ShapeDtypeStruct((n, *w.shape), w.dtype) for w in weights),
+        in_specs=[vmem] * 4,
+        out_specs=(vmem,) * 4,
+        scratch_shapes=[DMA((4,))]
+        + pairs((2, 2, n - 1), (2, 2, slots), (2, 2, 2, slots), (2, 4, n), (2, 2, n - 1)),
         compiler_params=pltpu.CompilerParams(
             collective_id=0, has_side_effects=True, vmem_limit_bytes=40 * 2**20
         ),
         name="gather_bases",
-    )(basis_q, basis_o, weight)
+    )(basis_q, basis_o, *weights)
 
 
 def second_kernel(
@@ -346,7 +367,7 @@
         for a in (1, 0):
             for k in (2, 1, 3):
                 swap(a, j, k).start()
-    weights.start(1)
+    weights.tick()
     final = [None, None]
     for j in range(1, n + 1):
         f = lax.rem(fs + j, n)
@@ -391,11 +412,7 @@
 
         return view
 
-    gather(n, [view_of(go_ref), view_of(gq_ref), view_of(gs)], (ls, lr), (os, orr), (ts, tr))
-    for step in range(1, n):
-        weights.arrive(step)
-        if step < n - 1:
-            weights.start(step + 1)
+    gather(n, [view_of(go_ref), view_of(gq_ref), view_of(gs)], (ls, lr), (os, orr), (ts, tr), ticks=[weights])
     tot_ref[0] = sum(gs[b] for b in range(4 * n))
     pair = remote(tot_ref.at[0], tot_ref.at[1], cs.at[0], cr.at[0], (fs, rep, 1 - tp))
     pair.start()
@@ -456,7 +473,9 @@
 ):
     f32, b16 = jnp.float32, jnp.bfloat16
     rank = query_basis.shape[1]
-    gq, go, wq = gather_bases(n, query_basis, output_basis, query_weight.astype(b16))
+    half = output_weight.shape[0] // 2
+    near, far = output_weight[:half].astype(b16), output_weight[half:].astype(b16)
+    gq, go, wq, wo_near = gather_bases(n, query_basis, output_basis, query_weight.astype(b16), near)
     whole_q, whole_o = gq.reshape(-1, rank), go.reshape(-1, rank)
 
     def project(inputs, basis, cotangent):
@@ -466,8 +485,8 @@
 
     part_q = project(query_input, whole_q, query_cotangent)
     part_o = project(branch_output, whole_o, layer_cotangent)
-    first_q, second_q, first_o, second_o, nq, no, wo, totals = advance(
-        n, part_q, part_o, query_first, query_second, output_first, output_second, output_weight.astype(b16)
+    first_q, second_q, first_o, second_o, nq, no, wo_far, totals = advance(
+        n, part_q, part_o, query_first, query_second, output_first, output_second, far
     )
     sums = jnp.sum(totals.reshape(16, 2, 128), axis=(0, 2))
     rep = lax.axis_index("rep")
@@ -484,7 +503,7 @@
         return mine, (weights.astype(f32) - step_rate * group).astype(b16)
 
     update_q, copy_q = update(query_basis, whole_q, nq, sums[0], wq)
-    update_o, copy_o = update(output_basis, whole_o, no, sums[1], wo)
+    update_o, copy_o = update(output_basis, whole_o, no, sums[1], jnp.concatenate([wo_near, wo_far], axis=1))
     return (update_q, update_o, first_q, second_q, first_o, second_o, copy_q, copy_o)
 
 

time: 189 us -> 177 us (0.937)
  Pallas kernels: 136 us -> 122 us
  other arithmetic: 1.36 us -> 4.22 us
    pallas_call x1, Pallas kernels: 83.8 us -> 65.4 us  [advance(): pl.pallas_call(functools.partial(second_kernel, n), out_shape=(shape((row...]
    pallas_call x1, Pallas kernels: 52.1 us -> 56.6 us  [gather_bases(): pl.pallas_call(functools.partial(first_kernel, n), out_shape=(whole(basis...]
    unnamed x52 -> x54, local copies, waits for them, and re-layouts: 16.5 us -> 15.5 us
where the time goes in v2:
time: 177 us; the launch traced here: 176 us
  Pallas kernels  122 us (69%)
  matrix products  31.9 us (18%)
  local copies, waits for them, and re-layouts  16.1 us (9%)
  other arithmetic  4.22 us (2%)
  between operations  2.24 us (1%)
    pallas_call x1, Pallas kernels, advance(): pl.pallas_call(functools.partial(second_kernel, n), out_shape=(shape((row...  65.4 us
    pallas_call x1, Pallas kernels, gather_bases(): pl.pallas_call(functools.partial(first_kernel, n), out_shape=(whole(basis...  56.6 us
    dot_general x2, matrix products, project(): lax.dot_general(inner, cotangent, (((0,), (0,)), ((), ())), preferred_ele...  20.9 us
    unnamed x54, local copies, waits for them, and re-layouts  15.5 us
    dot_general x2, matrix products, update(): group = scale * jnp.dot(rows, normed, preferred_element_type=f32)  7.88 us

profile of v2, /device:TPU:0, one launch (start us, length us, event | category | flops | bytes accessed | tf_op | source)
XLA Modules:
  0.0 176.4 jit_solution(659522946599924232)
XLA Ops:
  0.6 0.0 copy-start
  0.6 1.4 convert.6
  2.1 1.1 convert_element_type.37.w_ref
  3.2 0.0 copy-start.1
  3.2 0.9 copy-done.1
  4.1 0.0 copy-start.7
  4.1 0.9 copy-done.7
  5.0 56.6 %gather_bases.1 = (bf16[16,256,512]{2,1,0:T(8,128)(2,1)S(1)}, bf16[16,128,512]{2,1,0:T(8,128)(2,1)S(1)}, bf16[4,256,512]{2,1,0:T(8,128)(2,1)S(1)}, bf16[4,64,2048]{2,1,0:T(8,128)(2,1)S(1)}) custom-call(bf16[256,512]{1,0:T(8,128)(2,1)S(1)} %copy-done.1, bf16[128,512]{1,0:T(8,128)(2,1)S(1)} %copy-done.7, bf16[256,512]{1,0:T(8,128)(2,1)S(1)} %convert_element_type.37.w_ref, ...), custom_call_target="tpu_custom_call" | custom-call | tf_op jit(solution)/shard_map/gather_bases/pallas_call | solution.py:321
  61.6 0.0 copy-start.21
  61.6 1.9 %copy-done.21 = bf16[16,256,512]{2,1,0:T(8,128)(2,1)} copy-done((bf16[16,256,512]{2,1,0:T(8,128)(2,1)}, bf16[16,256,512]{2,1,0:T(8,128)(2,1)S(1)}, u32[]{:S(2)}) %copy-start.21) | copy-done | bytes 4194328
  63.6 0.0 copy-start.22
  63.6 1.3 copy-done.22
  64.9 0.0 copy-start.23
  64.9 1.0 copy-done.23
  65.9 0.0 copy-start.3
  65.9 10.3 %convolution_convert_fusion = bf16[512,2048]{1,0:T(8,128)(2,1)} fusion(bf16[1024,2048]{1,0:T(8,128)(2,1)} %param.15, bf16[2048,512]{1,0:T(8,128)(2,1)} %bitcast.37, bf16[1024,2048]{1,0:T(8,128)(2,1)} %param.14), kind=kOutput, calls=%fused_computation.2 | convolution fusion | flops 4296540160 | bytes 12582912 | tf_op jit(solution)/shard_map/dot_general | solution.py:483
  76.2 0.0 copy-done.3
  76.2 0.0 copy-done
  76.2 0.0 copy-start.15
  76.2 0.0 copy-start.16
  76.2 10.6 %convolution_convert_fusion.3 = bf16[512,512]{1,0:T(8,128)(2,1)} fusion(bf16[1024,512]{1,0:T(8,128)(2,1)S(1)} %copy-done, bf16[4096,512]{1,0:T(8,128)(2,1)} %bitcast.35, bf16[1024,4096]{1,0:T(8,128)(2,1)} %param.12), kind=kOutput, calls=%fused_computation.10 | convolution fusion | flops 4832624640 | bytes 14155776 | tf_op jit(solution)/shard_map/dot_general | solution.py:483
  86.8 0.0 copy-start.4
  86.8 0.0 copy-done.15
  86.8 0.0 copy-done.16
  86.8 0.0 copy-start.6
  86.8 1.1 copy-done.6
  87.9 0.0 copy-start.9
  87.9 0.9 copy-done.9
  88.9 0.0 copy-start.10
  88.9 0.9 copy-done.10
  89.8 65.4 %advance.1 = (f32[32,512]{1,0:T(8,128)S(1)}, f32[32,512]{1,0:T(8,128)S(1)}, f32[32,2048]{1,0:T(8,128)S(1)}, f32[32,2048]{1,0:T(8,128)S(1)}, bf16[16,32,512]{2,1,...) custom-call(bf16[16,32,512]{2,1,0:T(8,128)(2,1)S(1)} %bitcast.34, ...), custom_call_target="tpu_custom_call" | custom-call | tf_op jit(solution)/shard_map/advance/pallas_call | solution.py:436
  155.2 0.0 copy-start.5
  155.2 0.0 copy-start.11
  155.3 0.0 copy-start.13
  155.3 0.0 copy-start.17
  155.3 0.0 copy-start.19
  155.3 0.0 copy-done.4
  155.3 1.6 pad_maximum_fusion
  156.9 0.0 copy-done.5
  156.9 0.0 copy-done.11
  156.9 0.0 copy-done.13
  156.9 0.0 copy-done.17
  157.0 0.0 copy-done.19
  157.0 0.1 bitcast_reduce_fusion
  157.1 0.6 fusion.9
  158.4 4.4 %fusion = bf16[512,2048]{1,0:T(8,128)(2,1)} fusion(bf16[512,2048]{1,0:T(8,128)(2,1)} %bitcast.41, bf16[512,2048]{1,0:T(8,128)(2,1)S(1)} %bitcast.30, f32[]{:T(128)} %bitcast.8, bf16[2048,512]{1,0:T(8,128)(2,1)} %bitcast.38, s32[]{:T(128)S(6)} %select_n.7), kind=kOutput, calls=%fused_computation.1 | convolution fusion | flops 1078984704 | bytes 6816260 | tf_op jit(solution)/shard_map/dot_general | solution.py:502
  162.8 0.0 copy-start.8
  163.6 3.4 %fusion.2 = bf16[1024,512]{1,0:T(8,128)(2,1)} fusion(bf16[1024,512]{1,0:T(8,128)(2,1)} %bitcast.39, bf16[512,512]{1,0:T(8,128)(2,1)} %bitcast.32, bf16[4096,512]{1,0:T(8,128)(2,1)} %bitcast.36, s32[]{:T(128)S(6)} %select_n.6, f32[]{:T(128)} %bitcast.5), kind=kOutput, calls=%fused_computation.7 | convolution fusion | flops 539492352 | bytes 3670532 | tf_op jit(solution)/shard_map/dot_general | solution.py:502
  167.0 0.0 copy-done.8
  167.0 0.0 copy-start.2
  167.0 1.7 fusion.1
  168.7 0.0 copy-start.20
  168.8 2.6 %copy.23 = f32[128,2048]{1,0:T(8,128)} copy(f32[128,2048]{0,1:T(8,128)} %fusion.1) | data formatting | bytes 2097152
  171.4 0.0 copy-done.2
  171.4 1.4 fusion.3
  172.7 1.0 copy.22
  173.7 0.0 copy-done.20
  173.7 0.6 copy.28
  174.4 0.0 copy-done.18
  174.4 0.6 copy.29
  175.0 0.0 copy-done.14
  175.0 0.7 copy.30
  175.7 0.0 copy-done.12
  175.7 0.7 copy.31
  (5 shorter events, 0.1 us)
Async XLA Ops:
  0.6 75.6 %copy-start = (bf16[1024,512]{1,0:T(8,128)(2,1)S(1)}, bf16[1024,512]{1,0:T(8,128)(2,1)}, u32[]{:S(2)}) copy-start(bf16[1024,512]{1,0:T(8,128)(2,1)} %param.13) | copy-start | bytes 3145732
  3.2 1.0 copy-start.1
  4.1 0.9 copy-start.7
  61.6 1.9 %copy-start.21 = (bf16[16,256,512]{2,1,0:T(8,128)(2,1)}, bf16[16,256,512]{2,1,0:T(8,128)(2,1)S(1)}, u32[]{:S(2)}) copy-start(bf16[16,256,512]{2,1,0:T(8,128)(2,1)S(1)} %get-tuple-element.20) | copy-start | bytes 12582916
  63.6 1.3 copy-start.22
  64.9 1.0 copy-start.23
  65.9 10.3 %copy-start.3 = (bf16[4,64,2048]{2,1,0:T(8,128)(2,1)}, bf16[4,64,2048]{2,1,0:T(8,128)(2,1)S(1)}, u32[]{:S(2)}) copy-start(bf16[4,64,2048]{2,1,0:T(8,128)(2,1)S(1)} %get-tuple-element.30) | copy-start | bytes 3145732
  76.2 10.6 %copy-start.15 = (f32[32,512]{1,0:T(8,128)S(1)}, f32[32,512]{1,0:T(8,128)}, u32[]{:S(2)}) copy-start(f32[32,512]{1,0:T(8,128)} %fq_ref.1) | copy-start | bytes 196612
  76.2 10.6 %copy-start.16 = (f32[32,512]{1,0:T(8,128)S(1)}, f32[32,512]{1,0:T(8,128)}, u32[]{:S(2)}) copy-start(f32[32,512]{1,0:T(8,128)} %sq_ref.1) | copy-start | bytes 196612
  86.8 68.5 %copy-start.4 = (bf16[4,64,2048]{2,1,0:T(8,128)(2,1)S(1)}, bf16[4,64,2048]{2,1,0:T(8,128)(2,1)}, u32[]{:S(2)}) copy-start(bf16[4,64,2048]{2,1,0:T(8,128)(2,1)} %copy-done.3) | copy-start | bytes 3145732
  86.8 1.1 copy-start.6
  87.9 0.9 copy-start.9
  88.9 0.9 copy-start.10
  155.2 1.7 copy-start.5
  155.2 1.7 copy-start.11
  155.3 1.7 copy-start.13
  155.3 1.7 copy-start.17
  155.3 1.7 copy-start.19
  162.8 4.2 %copy-start.8 = (bf16[128,512]{1,0:T(8,128)(2,1)S(1)}, bf16[128,512]{1,0:T(8,128)(2,1)}, u32[]{:S(2)}) copy-start(bf16[128,512]{1,0:T(8,128)(2,1)} %bo_ref.1) | copy-start | bytes 393220
  167.0 4.4 %copy-start.2 = (bf16[256,512]{1,0:T(8,128)(2,1)S(1)}, bf16[256,512]{1,0:T(8,128)(2,1)}, u32[]{:S(2)}) copy-start(bf16[256,512]{1,0:T(8,128)(2,1)} %bq_ref.1) | copy-start | bytes 786436
  168.7 5.0 %copy-start.20 = (f32[32,512]{1,0:T(8,128)S(1)}, f32[32,512]{1,0:T(8,128)}, u32[]{:S(2)}) copy-start(f32[32,512]{1,0:T(8,128)} %copy-done.19) | copy-start | bytes 196612
  168.8 5.6 %copy-start.18 = (f32[32,512]{1,0:T(8,128)S(1)}, f32[32,512]{1,0:T(8,128)}, u32[]{:S(2)}) copy-start(f32[32,512]{1,0:T(8,128)} %copy-done.17) | copy-start | bytes 196612
  168.8 6.3 %copy-start.14 = (f32[32,2048]{1,0:T(8,128)S(1)}, f32[32,2048]{1,0:T(8,128)}, u32[]{:S(2)}) copy-start(f32[32,2048]{1,0:T(8,128)} %copy-done.13) | copy-start | bytes 786436
  168.8 7.0 %copy-start.12 = (f32[32,2048]{1,0:T(8,128)S(1)}, f32[32,2048]{1,0:T(8,128)}, u32[]{:S(2)}) copy-start(f32[32,2048]{1,0:T(8,128)} %copy-done.11) | copy-start | bytes 786436
